TPU v7x, 32 devices: a whole 2x2x4 slice. The times are simulated.
32 devices in a mesh: sp: 16 (over z, y, x), tp: 2 (over core).
Axes of the slice: x: 2, y: 2, z: 4, core: 2. Of those that a mesh axis runs over, the one named last changes fastest.
Arguments:
- queries: bfloat16 [1, 6144, 2048], P(None, 'sp', 'tp'), may hold values from -5 to 5
- keys: bfloat16 [1, 6144, 2048], P(None, 'sp', 'tp'), may hold values from -5 to 5
- values: bfloat16 [1, 6144, 2048], P(None, 'sp', 'tp'), may hold values from -6 to 6
- rel_bias: float32 [16, 192], P('tp'), may hold values from -3 to 3
- out_grad: bfloat16 [1, 6144, 2048], P(None, 'sp', 'tp'), may hold values from -48 to 48
Outputs:
- query_grad: bfloat16 [1, 6144, 2048], P(None, 'sp', 'tp')
- key_grad: bfloat16 [1, 6144, 2048], P(None, 'sp', 'tp')
- value_grad: bfloat16 [1, 6144, 2048], P(None, 'sp', 'tp')
- bias_grad: float32 [16, 192], replicated
All inputs are finite; a program needn't handle non-finite values.
Results may differ from a plain program's by a relative error of at most 0.0049.
Values may be sent and summed in bfloat16 or wider, within the bound.
A program may use at most 64 MiB of HBM per device.

v0:
```python
import jax
import jax.numpy as jnp
from jax import lax
from jax.sharding import PartitionSpec as P

HEAD_DIM = 128
SEG = 64
LEFT = 4
CLIP = 128
BAND = 320
BUCKETS = 192


def from_behind(value, axis, steps):
    count = lax.axis_size(axis)
    leading, last = (max(0, -steps), min(count, count - steps))
    return lax.ppermute(value, axis, [(source, source + steps) for source in range(leading, last)])


def diagonal_onehot():
    span = SEG + BAND - 1
    diag = jnp.arange(span, dtype=jnp.int32)
    bucket = jnp.clip(SEG - 1 - diag + LEFT * SEG, 1 - SEG, CLIP) + SEG - 1
    return (bucket[None, :] == jnp.arange(BUCKETS, dtype=jnp.int32)[:, None]).astype(jnp.float32)


def on_diagonals(rel_bias, onehot):
    return jnp.dot(
        rel_bias, onehot, preferred_element_type=jnp.float32, precision=lax.Precision.HIGHEST
    )


def fill_toeplitz(diag_vals):
    head_count, span = diag_vals.shape
    tiled = jnp.tile(diag_vals, (1, SEG))[:, SEG - 1 :]
    tiled = tiled[:, : SEG * (span - 1)].reshape(head_count, SEG, span - 1)
    return tiled[:, :, :BAND]


def sum_diagonals(terms):
    head_count = terms.shape[0]
    span = SEG + BAND - 1
    padded = jnp.concatenate(
        [
            jnp.zeros((head_count, SEG, SEG - 1), jnp.float32),
            terms,
            jnp.zeros((head_count, SEG, SEG), jnp.float32),
        ],
        axis=2,
    )
    width = padded.shape[2]
    flat = jnp.concatenate(
        [padded.reshape(head_count, SEG * width), jnp.zeros((head_count, SEG), jnp.float32)], axis=1
    )
    skewed = flat.reshape(head_count, SEG, width + 1)[:, :, :span]
    return jnp.sum(skewed, axis=1)


def band_core(q_segs, k_band, v_band, g_segs, table, key_valid):
    seg_count = q_segs.shape[1]
    score_scale = HEAD_DIM ** (-0.5)
    score_parts = []
    prob_parts = []
    for offset in range(LEFT + 1):
        score_parts.append(
            jnp.einsum(
                "sncha,snkha->snhck",
                q_segs,
                k_band[:, offset : offset + seg_count],
                preferred_element_type=jnp.float32,
            )
        )
        prob_parts.append(
            jnp.einsum(
                "sncha,snkha->snhck",
                g_segs,
                v_band[:, offset : offset + seg_count],
                preferred_element_type=jnp.float32,
            )
        )
    score = jnp.concatenate(score_parts, axis=-1) * score_scale + table[None, None]
    score = jnp.where(key_valid[None, :, None, None, :], score, -jnp.inf)
    row_max = jnp.max(score, axis=-1, keepdims=True)
    expo = jnp.exp(score - row_max)
    row_sum = jnp.sum(expo, axis=-1, keepdims=True)
    prob = expo / row_sum
    log_norm = (row_max + jnp.log(row_sum))[..., 0]
    prob_grad = jnp.concatenate(prob_parts, axis=-1)
    row_delta = jnp.sum(prob * prob_grad, axis=-1)
    score_grad = prob * (prob_grad - row_delta[..., None])
    bias_terms = jnp.sum(score_grad, axis=(0, 1))
    prob_low = prob.astype(jnp.bfloat16)
    grad_low = (score_grad * score_scale).astype(jnp.bfloat16)
    query_acc = jnp.zeros(q_segs.shape, jnp.float32)
    key_acc = jnp.zeros(k_band.shape, jnp.float32)
    value_acc = jnp.zeros(k_band.shape, jnp.float32)
    for offset in range(LEFT + 1):
        grad_part = grad_low[..., offset * SEG : (offset + 1) * SEG]
        prob_part = prob_low[..., offset * SEG : (offset + 1) * SEG]
        query_acc = query_acc + jnp.einsum(
            "snhck,snkha->sncha",
            grad_part,
            k_band[:, offset : offset + seg_count],
            preferred_element_type=jnp.float32,
        )
        first_seg = 0
        key_acc = key_acc.at[:, offset + first_seg : offset + seg_count].add(
            jnp.einsum("snhck,sncha->snkha", grad_part, q_segs, preferred_element_type=jnp.float32)
        )
        value_acc = value_acc.at[:, offset + first_seg : offset + seg_count].add(
            jnp.einsum("snhck,sncha->snkha", prob_part, g_segs, preferred_element_type=jnp.float32)
        )
    return (query_acc, key_acc, value_acc, bias_terms, log_norm, row_delta)


def local(queries, keys, values, rel_bias, out_grad):
    seq_count, tok_rows, row_width = queries.shape
    head_count = row_width // HEAD_DIM
    seg_count = tok_rows // SEG
    reach = LEFT * SEG
    seq_index = lax.axis_index("sp")
    seg_shape = (seq_count, seg_count, SEG, head_count, HEAD_DIM)
    band_shape = (seq_count, seg_count + LEFT, SEG, head_count, HEAD_DIM)
    onehot = diagonal_onehot()
    table = fill_toeplitz(on_diagonals(rel_bias, onehot))
    prior_k, prior_v = from_behind(
        (keys[:, tok_rows - reach :], values[:, tok_rows - reach :]), "sp", 1
    )
    k_band = jnp.concatenate([prior_k, keys], axis=1).reshape(band_shape)
    v_band = jnp.concatenate([prior_v, values], axis=1).reshape(band_shape)
    q_segs = queries.reshape(seg_shape)
    g_segs = out_grad.reshape(seg_shape)
    positions = (
        seq_index * tok_rows
        + jnp.arange(seg_count, dtype=jnp.int32)[:, None] * SEG
        - reach
        + jnp.arange(BAND, dtype=jnp.int32)[None, :]
    )
    key_valid = positions >= 0
    flat = (seq_count, reach + tok_rows, row_width)
    query_acc, key_acc, value_acc, bias_terms, log_norm, row_delta = band_core(
        q_segs, k_band, v_band, g_segs, table, key_valid
    )
    key_flat = key_acc.reshape(flat)
    value_flat = value_acc.reshape(flat)
    back_k, back_v = from_behind((key_flat[:, :reach], value_flat[:, :reach]), "sp", -1)
    key_own = key_flat[:, reach:].at[:, tok_rows - reach :].add(back_k)
    value_own = value_flat[:, reach:].at[:, tok_rows - reach :].add(back_v)
    query_grad = query_acc.astype(jnp.bfloat16).reshape(seq_count, tok_rows, row_width)
    key_grad = key_own.astype(jnp.bfloat16)
    value_grad = value_own.astype(jnp.bfloat16)
    local_bias = jnp.dot(
        sum_diagonals(bias_terms),
        onehot.T,
        preferred_element_type=jnp.float32,
        precision=lax.Precision.HIGHEST,
    )
    full_table = jnp.zeros((head_count * lax.axis_size("tp"), BUCKETS), jnp.float32)
    full_table = lax.dynamic_update_slice_in_dim(
        full_table, local_bias, lax.axis_index("tp") * head_count, 0
    )
    bias_grad = lax.psum(full_table, ("sp", "tp"))
    return (query_grad, key_grad, value_grad, bias_grad)


def solution(mesh):
    return jax.shard_map(
        local,
        mesh=mesh,
        in_specs=(
            P(None, "sp", "tp"),
            P(None, "sp", "tp"),
            P(None, "sp", "tp"),
            P("tp", None),
            P(None, "sp", "tp"),
        ),
        out_specs=(P(None, "sp", "tp"), P(None, "sp", "tp"), P(None, "sp", "tp"), P()),
        check_vma=False,
    )
```

profile of v0, /device:TPU:0, one launch (start us, length us, event | category | flops | bytes accessed | tf_op | source)
XLA Modules:
  0.0 184.4 jit_solution(14857570000628562760)
XLA Ops:
  0.7 2.0 %slice.478 = bf16[1,256,1024]{2,1,0:T(8,128)(2,1)} slice(bf16[1,384,1024]{2,1,0:T(8,128)(2,1)} %param.30), slice={[0:1], [128:384], [0:1024]} | slice | bytes 1048576 | tf_op jit(solution)/shard_map/slice | solution.py:127
  2.7 5.7 %collective-permute-start = (bf16[1,256,1024]{2,1,0:T(8,128)(2,1)}, bf16[1,256,1024]{2,1,0:T(8,128)(2,1)}, u32[]{:S(2)}, u32[]{:S(2)}) collective-permute-start(bf16[1,256,1024]{2,1,0:T(8,128)(2,1)} %slice.478), channel_id=1, source_target_pairs={{0,2},{2,4},{4,6},{6,8},{8,10},{10,12},{12,14},{14,16},{16,18},{18... | collective-permute-start | bytes 1572872 | tf_op jit(solution)/shard_map/ppermute | solution.py:17
  8.3 1.9 %slice.486 = bf16[1,256,1024]{2,1,0:T(8,128)(2,1)} slice(bf16[1,384,1024]{2,1,0:T(8,128)(2,1)} %param.31), slice={[0:1], [128:384], [0:1024]} | slice | bytes 1048576 | tf_op jit(solution)/shard_map/slice | solution.py:127
  10.2 3.4 %collective-permute-start.1 = (bf16[1,256,1024]{2,1,0:T(8,128)(2,1)}, bf16[1,256,1024]{2,1,0:T(8,128)(2,1)}, u32[]{:S(2)}, u32[]{:S(2)}) collective-permute-start(bf16[1,256,1024]{2,1,0:T(8,128)(2,1)} %slice.486), channel_id=1, source_target_pairs={{0,2},{2,4},{4,6},{6,8},{8,10},{10,12},{12,14},{14,16},{16,18},{18... | collective-permute-start | bytes 1572872 | tf_op jit(solution)/shard_map/ppermute | solution.py:17
  14.8 1.1 slice.522
  16.0 2.0 %reshape.1124 = f32[8,64,382]{2,1,0:T(8,128)S(1)} reshape(f32[8,24448]{1,0:T(8,128)} %slice.522) | data formatting | bytes 1564672 | tf_op jit(solution)/shard_map/reshape | solution.py:36
  18.1 2.1 %collective-permute-done = bf16[1,256,1024]{2,1,0:T(8,128)(2,1)} collective-permute-done((bf16[1,256,1024]{2,1,0:T(8,128)(2,1)}, bf16[1,256,1024]{2,1,0:T(8,128)(2,1)}, u32[]{:S(2)}, u32[]{:S(2)}) %collective-permute-start) | collective-permute-done | bytes 524320 | tf_op jit(solution)/shard_map/ppermute | solution.py:17
  20.1 1.4 maximum_bitcast_fusion
  22.8 7.4 %collective-permute-done.1 = bf16[1,256,1024]{2,1,0:T(8,128)(2,1)} collective-permute-done((bf16[1,256,1024]{2,1,0:T(8,128)(2,1)}, bf16[1,256,1024]{2,1,0:T(8,128)(2,1)}, u32[]{:S(2)}, u32[]{:S(2)}) %collective-permute-start.1) | collective-permute-done | bytes 524320 | tf_op jit(solution)/shard_map/ppermute | solution.py:17
  30.2 1.2 maximum_bitcast_fusion.1
  32.6 1.7 convolution_bitcast_fusion.6
  34.3 1.7 convolution_bitcast_fusion.5
  36.1 1.7 convolution_bitcast_fusion.4
  37.8 1.7 convolution_bitcast_fusion.3
  39.5 1.7 convolution_bitcast_fusion.2
  41.1 1.7 convolution_bitcast_fusion.11
  42.9 1.7 convolution_bitcast_fusion.10
  44.5 1.8 convolution_bitcast_fusion.9
  46.3 1.7 convolution_bitcast_fusion.8
  48.0 1.7 convolution_bitcast_fusion.7
  49.7 6.9 %concatenate.116 = f32[1,6,8,64,320]{4,3,2,1,0:T(8,128)} concatenate(f32[1,6,8,64,64]{4,3,2,1,0:T(8,128)} %convolution_bitcast_fusion.11, f32[1,6,8,64,64]{4,3,2,1,0:T(8,128)} %convolution_bitcast_fusion.10, f32[1,6,8,64,64]{4,3,2,1,0:T(8,128)} %convolution_bitcast_fusion.9, f32[1,6,8,64,64]{4,3,2,1,0:T(8,128)} %convolution_bitcast_fusion.8, ...), dimensions={4} | concatenate | bytes 7864320 | tf_op jit(solution)/shard_map/concatenate | solution.py:81
  56.7 3.4 %fusion.2 = f32[6,8,64]{2,1,0:T(8,128)S(1)} fusion(f32[1,6,8,64,320]{4,3,2,1,0:T(8,128)} %concatenate.116, f32[8,64,320]{2,1,0:T(8,128)S(1)} %bitcast.227, pred[6,320]{1,0:T(8,128)(4,1)S(1)} %add_compare_fusion), kind=kLoop, calls=%fused_computation.7 | loop fusion | flops 3929088 | bytes 4601728 | tf_op jit(solution)/shard_map/reduce_max | solution.py:83
  60.4 1.6 fusion.1
  62.1 7.0 %concatenate.123 = f32[1,6,8,64,320]{4,3,2,1,0:T(8,128)} concatenate(f32[1,6,8,64,64]{4,3,2,1,0:T(8,128)} %convolution_bitcast_fusion.6, f32[1,6,8,64,64]{4,3,2,1,0:T(8,128)} %convolution_bitcast_fusion.5, f32[1,6,8,64,64]{4,3,2,1,0:T(8,128)} %convolution_bitcast_fusion.4, f32[1,6,8,64,64]{4,3,2,1,0:T(8,128)} %convolution_bitcast_fusion.3, ...), dimensions={4} | concatenate | bytes 7864320 | tf_op jit(solution)/shard_map/concatenate | solution.py:88
  69.1 4.9 %multiply_reduce_fusion = f32[6,8,64]{2,1,0:T(8,128)S(1)} fusion(f32[1,6,8,64,320]{4,3,2,1,0:T(8,128)} %concatenate.123, f32[6,8,64]{2,1,0:T(8,128)S(1)} %fusion.1, f32[6,8,64]{2,1,0:T(8,128)S(1)} %fusion.2, f32[8,64,320]{2,1,0:T(8,128)S(1)} %bitcast.229, f32[1,6,8,64,320]{4,3,2,1,0:T(8,128)} %concatenate.116, pred[6,320]{1,0:T(8,128)(4,1)S(1)} %add_compare_fusion), kind=kLoop, calls=%fused_computation.2 | loop fusion | flops 6878208 | bytes 8558464 | tf_op jit(solution)/shard_map/reduce_sum | solution.py:89
  74.2 5.5 %fusion.3 = (f32[8,64,320]{2,1,0:T(8,128)}, bf16[1,6,8,64,320]{4,3,2,1,0:T(8,128)(2,1)S(1)}, bf16[1,6,8,64,320]{4,3,2,1,0:T(8,128)(2,1)S(1)}) fusion(f32[1,6,8,64,320]{4,3,2,1,0:T(8,128)S(1)} %copy-done.3, f32[6,8,64]{2,1,0:T(8,128)S(1)} %multiply_reduce_fusion, f32[6,8,64]{2,1,0:T(8,128)S(1)} %fusion.1, f32[6,8,64]{2,1,0:T(8,128)S(1)} %fusion.2, ...), kind=kLoop, calls=%fused_computation.8 | loop fusion | flops 10649600 | bytes 13145984 | tf_op jit(solution)/shard_map/reduce_sum | solution.py:91
  82.3 1.0 fusion.11
  85.7 1.6 copy.115
  87.3 1.7 slice.539
  89.1 1.5 collective-permute-start.2
  91.3 1.0 fusion.10
  95.6 1.6 copy.126
  97.3 1.8 slice.550
  99.1 1.5 collective-permute-start.3
  101.3 2.3 %slice.537 = bf16[1,384,1024]{2,0,1:T(2,128)(2,1)} slice(f32[1,640,1024]{2,0,1:T(1,128)S(1)} %bitcast.232), slice={[0:1], [256:640], [0:1024]} | slice | bytes 1572864 | tf_op jit(solution)/shard_map/slice | solution.py:147
  103.6 2.2 %slice.548 = bf16[1,384,1024]{2,0,1:T(2,128)(2,1)} slice(f32[1,640,1024]{2,0,1:T(1,128)S(1)} %bitcast.235), slice={[0:1], [256:640], [0:1024]} | slice | bytes 1572864 | tf_op jit(solution)/shard_map/slice | solution.py:148
  105.8 1.4 copy.104
  107.2 2.1 %reshape.1137 = bf16[1,384,1024]{2,1,0:T(8,128)(2,1)} reshape(bf16[1,6,64,8,128]{4,3,2,1,0:T(8,128)(2,1)} %copy.104) | data formatting | bytes 1572864 | tf_op jit(solution)/shard_map/reshape | solution.py:149
  109.4 1.3 maximum_maximum_fusion
  110.7 2.7 %reshape.1155 = f32[8,28608]{1,0:T(8,128)} reshape(f32[8,64,447]{2,1,0:T(8,128)} %maximum_maximum_fusion) | data formatting | bytes 1830912 | tf_op jit(solution)/shard_map/reshape | solution.py:53
  113.4 2.2 %concatenate.125 = f32[8,28672]{1,0:T(8,128)} pad(f32[8,28608]{1,0:T(8,128)} %reshape.1155, f32[]{:T(128)} %constant.322.clone.1), padding=0_0x0_64 | pad | bytes 1832964 | tf_op jit(solution)/shard_map/concatenate | solution.py:52
  115.6 2.7 %reshape.1156 = f32[8,64,448]{2,1,0:T(8,128)} reshape(f32[8,28672]{1,0:T(8,128)} %concatenate.125) | data formatting | bytes 1835008 | tf_op jit(solution)/shard_map/reshape | solution.py:55
  118.3 1.2 slice_reduce_fusion
  119.7 54.4 %psum.7 = f32[16,192]{1,0:T(8,128)} all-reduce(f32[16,192]{1,0:T(8,128)S(1)} %convolution_dynamic-update-slice_fusion), channel_id=1, replica_groups=mesh['sp'=16,'tp'=2] {'sp','tp'}, use_global_device_ids=true, to_apply=%region_5.6 | all-reduce | flops 3072 | bytes 24576 | tf_op jit(solution)/shard_map/psum | solution.py:162
  174.1 3.8 %fusion.14 = bf16[1,384,1024]{2,0,1:T(2,128)(2,1)} fusion(bf16[1,384,1024]{2,0,1:T(2,128)(2,1)} %slice.537, f32[1,256,1024]{2,0,1:T(1,128)} %collective-permute-done.2, f32[1,640,1024]{2,0,1:T(1,128)S(1)} %bitcast.233), kind=kLoop, calls=%fused_computation.46 | loop fusion | flops 262144 | bytes 3145728 | tf_op jit(solution)/shard_map/scatter-add | solution.py:147
  177.9 2.6 %copy.127 = bf16[1,384,1024]{2,1,0:T(8,128)(2,1)} copy(bf16[1,384,1024]{2,0,1:T(2,128)(2,1)} %fusion.14) | data formatting | bytes 1572864
  180.5 2.7 %fusion.13 = bf16[1,384,1024]{2,0,1:T(2,128)(2,1)S(1)} fusion(bf16[1,384,1024]{2,0,1:T(2,128)(2,1)S(1)} %copy-done.13, f32[1,256,1024]{2,0,1:T(1,128)} %collective-permute-done.3, f32[1,640,1024]{2,0,1:T(1,128)} %bitcast.236), kind=kLoop, calls=%fused_computation.44 | loop fusion | flops 262144 | bytes 3145728 | tf_op jit(solution)/shard_map/scatter-add | solution.py:148
  183.2 1.2 copy.128
  (71 shorter events, 14.2 us)
Async XLA Ops:
  0.6 13.0 %copy-start = (f32[8,192]{1,0:T(8,128)S(1)}, f32[8,192]{1,0:T(8,128)}, u32[]{:S(2)}) copy-start(f32[8,192]{1,0:T(8,128)} %param.32) | copy-start | bytes 18436
  0.6 13.2 %copy-start.16 = (bf16[1,384,1024]{2,1,0:T(8,128)(2,1)S(1)}, bf16[1,384,1024]{2,1,0:T(8,128)(2,1)}, u32[]{:S(2)}) copy-start(bf16[1,384,1024]{2,1,0:T(8,128)(2,1)} %param.33) | copy-start | bytes 2359300
  0.7 13.4 %copy-start.17 = (bf16[1,384,1024]{2,1,0:T(8,128)(2,1)S(1)}, bf16[1,384,1024]{2,1,0:T(8,128)(2,1)}, u32[]{:S(2)}) copy-start(bf16[1,384,1024]{2,1,0:T(8,128)(2,1)} %param.29) | copy-start | bytes 2359300
  2.7 17.5 %collective-permute-start = (bf16[1,256,1024]{2,1,0:T(8,128)(2,1)}, bf16[1,256,1024]{2,1,0:T(8,128)(2,1)}, u32[]{:S(2)}, u32[]{:S(2)}) collective-permute-start(bf16[1,256,1024]{2,1,0:T(8,128)(2,1)} %slice.478), channel_id=1, source_target_pairs={{0,2},{2,4},{4,6},{6,8},{8,10},{10,12},{12,14},{14,16},{16,18},{18... | collective-permute-start | bytes 1572872 | tf_op jit(solution)/shard_map/ppermute | solution.py:17
  10.2 20.0 %collective-permute-start.1 = (bf16[1,256,1024]{2,1,0:T(8,128)(2,1)}, bf16[1,256,1024]{2,1,0:T(8,128)(2,1)}, u32[]{:S(2)}, u32[]{:S(2)}) collective-permute-start(bf16[1,256,1024]{2,1,0:T(8,128)(2,1)} %slice.486), channel_id=1, source_target_pairs={{0,2},{2,4},{4,6},{6,8},{8,10},{10,12},{12,14},{14,16},{16,18},{18... | collective-permute-start | bytes 1572872 | tf_op jit(solution)/shard_map/ppermute | solution.py:17
  21.9 8.4 %copy-start.15 = (bf16[1,384,1024]{2,1,0:T(8,128)(2,1)S(1)}, bf16[1,384,1024]{2,1,0:T(8,128)(2,1)}, u32[]{:S(2)}) copy-start(bf16[1,384,1024]{2,1,0:T(8,128)(2,1)} %param.31) | copy-start | bytes 2359300
  22.8 20.1 %copy-start.7 = (bf16[1,6,64,8,128]{4,3,2,1,0:T(8,128)(2,1)}, bf16[1,6,64,8,128]{4,3,2,1,0:T(8,128)(2,1)S(1)}, u32[]{:S(2)}) copy-start(bf16[1,6,64,8,128]{4,3,2,1,0:T(8,128)(2,1)S(1)} %get-tuple-element.162) | copy-start | bytes 2359300
  22.8 21.8 %copy-start.9 = (bf16[1,6,64,8,128]{4,3,2,1,0:T(8,128)(2,1)}, bf16[1,6,64,8,128]{4,3,2,1,0:T(8,128)(2,1)S(1)}, u32[]{:S(2)}) copy-start(bf16[1,6,64,8,128]{4,3,2,1,0:T(8,128)(2,1)S(1)} %get-tuple-element.161) | copy-start | bytes 2359300
  22.8 23.5 %copy-start.11 = (bf16[1,6,64,8,128]{4,3,2,1,0:T(8,128)(2,1)}, bf16[1,6,64,8,128]{4,3,2,1,0:T(8,128)(2,1)S(1)}, u32[]{:S(2)}) copy-start(bf16[1,6,64,8,128]{4,3,2,1,0:T(8,128)(2,1)S(1)} %get-tuple-element.160) | copy-start | bytes 2359300
  22.8 25.3 %copy-start.5 = (bf16[1,6,64,8,128]{4,3,2,1,0:T(8,128)(2,1)}, bf16[1,6,64,8,128]{4,3,2,1,0:T(8,128)(2,1)S(1)}, u32[]{:S(2)}) copy-start(bf16[1,6,64,8,128]{4,3,2,1,0:T(8,128)(2,1)S(1)} %get-tuple-element.159) | copy-start | bytes 2359300
  56.7 3.8 %copy-start.2 = (f32[1,6,8,64,320]{4,3,2,1,0:T(8,128)S(1)}, f32[1,6,8,64,320]{4,3,2,1,0:T(8,128)}, u32[]{:S(2)}) copy-start(f32[1,6,8,64,320]{4,3,2,1,0:T(8,128)} %concatenate.116) | copy-start | bytes 11796484
  69.1 5.1 %copy-start.3 = (f32[1,6,8,64,320]{4,3,2,1,0:T(8,128)S(1)}, f32[1,6,8,64,320]{4,3,2,1,0:T(8,128)}, u32[]{:S(2)}) copy-start(f32[1,6,8,64,320]{4,3,2,1,0:T(8,128)} %concatenate.123) | copy-start | bytes 11796484
  74.2 5.5 %copy-start.12 = (bf16[1,6,64,8,128]{4,3,2,1,0:T(8,128)(2,1)S(1)}, bf16[1,6,64,8,128]{4,3,2,1,0:T(8,128)(2,1)}, u32[]{:S(2)}) copy-start(bf16[1,6,64,8,128]{4,3,2,1,0:T(8,128)(2,1)} %copy-done.11) | copy-start | bytes 2359300
  79.7 1.1 copy-start.10
  89.1 85.1 %collective-permute-start.2 = (f32[1,256,1024]{2,0,1:T(1,128)}, f32[1,256,1024]{2,0,1:T(1,128)}, u32[]{:S(2)}, u32[]{:S(2)}) collective-permute-start(f32[1,256,1024]{2,0,1:T(1,128)} %slice.539), channel_id=1, source_target_pairs={{2,0},{4,2},{6,4},{8,6},{10,8},{12,10},{14,12},{16,14},{18,16},{20... | collective-permute-start | bytes 3145736 | tf_op jit(solution)/shard_map/ppermute | solution.py:17
  94.1 1.1 copy-start.8
  97.3 6.3 %copy-start.4 = (f32[1,10,64,8,128]{4,3,0,2,1:T(8,128)}, f32[1,10,64,8,128]{4,3,0,2,1:T(8,128)S(1)}, u32[]{:S(2)}) copy-start(f32[1,10,64,8,128]{4,3,0,2,1:T(8,128)S(1)} %copy.126) | copy-start | bytes 7864324
  97.3 3.4 %copy-start.6 = (bf16[1,6,64,8,128]{4,3,2,1,0:T(8,128)(2,1)S(1)}, bf16[1,6,64,8,128]{4,3,2,1,0:T(8,128)(2,1)}, u32[]{:S(2)}) copy-start(bf16[1,6,64,8,128]{4,3,2,1,0:T(8,128)(2,1)} %copy-done.5) | copy-start | bytes 2359300
  99.1 81.4 %collective-permute-start.3 = (f32[1,256,1024]{2,0,1:T(1,128)}, f32[1,256,1024]{2,0,1:T(1,128)}, u32[]{:S(2)}, u32[]{:S(2)}) collective-permute-start(f32[1,256,1024]{2,0,1:T(1,128)} %slice.550), channel_id=1, source_target_pairs={{2,0},{4,2},{6,4},{8,6},{10,8},{12,10},{14,12},{16,14},{18,16},{20... | collective-permute-start | bytes 3145736 | tf_op jit(solution)/shard_map/ppermute | solution.py:17
  105.8 3.5 %copy-start.14 = (f32[8,64,320]{2,1,0:T(8,128)S(1)}, f32[8,64,320]{2,1,0:T(8,128)}, u32[]{:S(2)}) copy-start(f32[8,64,320]{2,1,0:T(8,128)} %get-tuple-element.156) | copy-start | bytes 1966084
  174.1 6.4 %copy-start.13 = (bf16[1,384,1024]{2,0,1:T(2,128)(2,1)S(1)}, bf16[1,384,1024]{2,0,1:T(2,128)(2,1)}, u32[]{:S(2)}) copy-start(bf16[1,384,1024]{2,0,1:T(2,128)(2,1)} %slice.548) | copy-start | bytes 2359300
  177.9 6.4 %copy-start.1 = (f32[8,192]{1,0:T(8,128)S(1)}, f32[8,192]{1,0:T(8,128)}, u32[]{:S(2)}) copy-start(f32[8,192]{1,0:T(8,128)} %param.32) | copy-start | bytes 18436
where the time goes:
time: 185 us; the launch traced here: 184 us
  blocking collectives  54.4 us (29%)
  local copies, waits for them, and re-layouts  52.7 us (28%)
  matrix products  27.5 us (15%)
  other arithmetic  27.1 us (15%)
  starting transfers between devices  12.1 us (7%)
  waiting for transfers between devices  9.53 us (5%)
    psum x1, blocking collectives, local(): bias_grad = lax.psum(full_table, ('sp', 'tp'))  54.4 us
    ppermute x4, starting transfers between devices, from_behind(): lax.ppermute(value, axis, [(source, source + steps) for source in range(l...  12.1 us
    ppermute x4, waiting for transfers between devices, from_behind(): lax.ppermute(value, axis, [(source, source + steps) for source in range(l...  9.53 us
    dot_general x5, matrix products, band_core(): jnp.einsum('sncha,snkha->snhck', q_segs, k_band[:, offset:offset + seg_co...  8.59 us
    dot_general x5, matrix products, band_core(): jnp.einsum('sncha,snkha->snhck', g_segs, v_band[:, offset:offset + seg_co...  8.5 us
    concatenate x1, local copies, waits for them, and re-layouts, band_core(): prob_grad = jnp.concatenate(prob_parts, axis=-1)  7.01 us
    concatenate x1, local copies, waits for them, and re-layouts, band_core(): jnp.concatenate(score_parts, axis=-1) * score_scale + table[None, None]  6.93 us
    unnamed x42, local copies, waits for them, and re-layouts  6.5 us
  transfers between devices with their start and end apart: 4, of which 2 were waited for; matrix products, arithmetic and copies ran while one was open for 23% of the time, Pallas kernels for 0%

commit v1 on v0

v1 whole, which is shorter than its diff:
```python
import functools

import jax
import jax.numpy as jnp
from jax import lax
from jax.experimental import pallas as pl
from jax.experimental.pallas import tpu as pltpu
from jax.sharding import PartitionSpec as P

HEAD_DIM = 128
SEG = 64
LEFT = 4
BUCKETS = 192
TILE = 2 * SEG
REACH = LEFT * SEG
SPAN = REACH + TILE
LANES = 256
LOW = -1e30
SCALE = HEAD_DIM ** (-0.5)
MESH = pl.DeviceIdType.MESH
F32 = jnp.float32
BF16 = jnp.bfloat16

NT = (((1,), (1,)), ((), ()))
TN = (((0,), (0,)), ((), ()))
NN = (((1,), (0,)), ((), ()))


def dot(a, b, dims):
    return lax.dot_general(a, b, dims, preferred_element_type=F32)


def toeplitz(row):
    x = jnp.broadcast_to(row, (8, LANES))
    x = pltpu.roll(x, LANES - (SEG - 1), axis=1)
    sub = lax.broadcasted_iota(jnp.int32, (8, LANES), 0)
    for bit in (1, 2, 4):
        x = jnp.where((sub & bit) != 0, pltpu.roll(x, bit, axis=1), x)
    rows = 8
    while rows < TILE:
        x = jnp.concatenate([x, pltpu.roll(x, rows, axis=1)], axis=0)
        rows *= 2
    return x


def skew_sum(z):
    rows = TILE
    while rows > 8:
        half = rows // 2
        z = z[:half] + pltpu.roll(z[half:], LANES - half, axis=1)
        rows = half
    for half in (4, 2, 1):
        z = z + pltpu.roll(pltpu.roll(z, 8 - half, axis=0), LANES - half, axis=1)
    return pltpu.roll(z, SEG - 1, axis=1)[0:1]


def partial_stats(s, dp):
    m = jnp.max(s, axis=0, keepdims=True)
    e = jnp.exp(s - m)
    return e, m, jnp.sum(e, axis=0, keepdims=True), jnp.sum(e * dp, axis=0, keepdims=True)


def merged(e, dp, mine, other):
    m, l, d = mine
    mo, lo, do = other
    top = jnp.maximum(m, mo)
    c, co = jnp.exp(m - top), jnp.exp(mo - top)
    inv = 1.0 / (l * c + lo * co)
    delta = (d * c + do * co) * inv
    p = e * (c * inv)
    return p, p * (dp - delta)


def pack(a, b):
    zero = jnp.zeros((2, TILE), F32)
    return jnp.concatenate([*a, *b, zero], axis=0)


def unpack(st):
    rows = [st[i : i + 1] for i in range(6)]
    return rows[:3], rows[3:]


def kernel(
    sp_n, tp_n, low_n, heads, tok,
    q_hbm, k_hbm, v_hbm, g_hbm, rb_ref,
    dq_hbm, dk_hbm, dv_hbm, bias_ref,
    q, k, v, g, dqo, dko, dvo, rq, rg, rbp, table, gsum, acck, accv, es, dps,
    st_own, st_next, st_half, st_prev, dq_loc, dq_out, dq_in,
    b0, b1, b2, slots1, slots2, slots3,
    in_sem, q_s, q_r, g_s, g_r, so_s, so_r, sh_s, sh_r, dq_s, dq_r,
    e1_s, e1_r, e2_s, e2_r, e3_s, e3_r, kv_sem, dqo_sem,
):
    sp = lax.axis_index("sp")
    tp = lax.axis_index("tp")
    high_n = sp_n // low_n
    low, high = lax.rem(sp, low_n), lax.div(sp, low_n)
    has_prev = sp > 0
    has_next = sp < sp_n - 1
    groups = tok // TILE
    lead = min(3, heads)
    half_heads = heads // 2

    def cols_of(h):
        return pl.ds(pl.multiple_of(h * HEAD_DIM, HEAD_DIM), HEAD_DIM)

    loads = [
        pltpu.make_async_copy(src.at[0], dst, in_sem.at[i])
        for i, (src, dst) in enumerate(((q_hbm, q), (k_hbm, k), (g_hbm, g), (v_hbm, v)))
    ]
    for load in loads:
        load.start()

    barrier = pltpu.get_barrier_semaphore()

    def greet(axis, index):
        pl.semaphore_signal(barrier, inc=1, device_id={axis: index}, device_id_type=MESH)

    @pl.when(has_prev)
    def _():
        greet("sp", sp - 1)

    @pl.when(has_next)
    def _():
        greet("sp", sp + 1)

    for d in range(1, low_n):
        greet("sp", high * low_n + lax.rem(low + d, low_n))
    for d in range(1, high_n):
        greet("sp", lax.rem(high + d, high_n) * low_n + low)
    for d in range(1, tp_n):
        greet("tp", lax.rem(tp + d, tp_n))
    ends = (sp == 0).astype(jnp.int32) + (sp == sp_n - 1).astype(jnp.int32)
    pl.semaphore_wait(barrier, low_n + high_n + tp_n - 1 - ends)

    def q_copy(h):
        return pltpu.make_async_remote_copy(
            q_hbm.at[0, pl.ds(0, REACH), cols_of(h)], rq.at[h], q_s.at[h], q_r.at[h],
            device_id={"sp": sp - 1}, device_id_type=MESH)

    def g_copy(h):
        return pltpu.make_async_remote_copy(
            g_hbm.at[0, pl.ds(0, REACH), cols_of(h)], rg.at[h], g_s.at[h], g_r.at[h],
            device_id={"sp": sp - 1}, device_id_type=MESH)

    own_copy = pltpu.make_async_remote_copy(
        st_own, st_next, so_s.at[0], so_r.at[0], device_id={"sp": sp - 1}, device_id_type=MESH)

    def half_copy(h):
        return pltpu.make_async_remote_copy(
            st_half.at[h], st_prev.at[h], sh_s.at[h], sh_r.at[h],
            device_id={"sp": sp + 1}, device_id_type=MESH)

    def dq_copy(h):
        return pltpu.make_async_remote_copy(
            dq_out.at[h], dq_in.at[h], dq_s.at[h], dq_r.at[h],
            device_id={"sp": sp + 1}, device_id_type=MESH)

    @pl.when(has_prev)
    def _():
        @pl.loop(0, lead)
        def _(h):
            q_copy(h).start()
            g_copy(h).start()

    row_b = lax.broadcasted_iota(jnp.int32, (TILE, TILE), 0)
    col_r = lax.broadcasted_iota(jnp.int32, (TILE, TILE), 1)
    far_ok = (col_r < SEG) | (row_b >= SEG)
    diag_ok = (row_b < SEG) | (col_r >= SEG)
    beyond = col_r >= row_b
    lane = lax.broadcasted_iota(jnp.int32, (1, LANES), 1)

    rbp[...] = jnp.zeros_like(rbp)
    rbp[0:heads, 0:BUCKETS] = rb_ref[...]
    b0[...] = jnp.zeros_like(b0)

    for load in loads:
        load.wait()

    @pl.loop(0, heads)
    def _(h):
        cols = cols_of(h)
        row = rbp[pl.ds(h, 1), :]
        last = jnp.sum(jnp.where(lane == BUCKETS - 1, row, 0.0), axis=1, keepdims=True)
        both = toeplitz(row)
        far = jnp.where(far_ok, jnp.broadcast_to(last, (TILE, TILE)), LOW)
        mid = jnp.where(beyond, jnp.broadcast_to(last, (TILE, TILE)), both[:, TILE:])
        diag = jnp.where(diag_ok, both[:, :TILE], LOW)
        tab = jnp.concatenate([far, mid, diag], axis=0)
        table[h] = tab

        def tiles(group, keys_from, tab_part):
            size = tab_part.shape[0]
            rows = slice(group * TILE, (group + 1) * TILE)
            keys = slice(keys_from, keys_from + size)
            s = dot(k[keys, cols], q[rows, cols], NT) * SCALE + tab_part
            dp = dot(v[keys, cols], g[rows, cols], NT)
            return s, dp

        s, dp = tiles(0, 0, diag)
        e0, *st0 = partial_stats(s, dp)
        es[h, 0:TILE] = e0
        dps[h, 0:TILE] = dp
        s, dp = tiles(1, 0, tab[TILE:])
        e1, *st1 = partial_stats(s, dp)
        es[h, TILE:SPAN] = e1
        dps[h, TILE:SPAN] = dp
        st_own[h] = pack(st0, st1)

        for group in range(2, groups):
            start = (group - 2) * TILE
            rows = slice(group * TILE, (group + 1) * TILE)
            keys = slice(start, start + SPAN)
            s, dp = tiles(group, start, tab)
            e, m, l, d = partial_stats(s, dp)
            inv = 1.0 / l
            p = e * inv
            sg = p * (dp - d * inv)
            low_p = p.astype(BF16)
            low_g = (sg * SCALE).astype(BF16)
            part_k = dot(low_g, q[rows, cols], NN)
            part_v = dot(low_p, g[rows, cols], NN)
            if group == 2:
                gsum[h] = sg
                acck[h, 0:SPAN] = part_k
                accv[h, 0:SPAN] = part_v
            else:
                gsum[h] += sg
                old = slice(start, start + REACH)
                new = slice(start + REACH, start + SPAN)
                acck[h, old] += part_k[:REACH]
                accv[h, old] += part_v[:REACH]
                acck[h, new] = part_k[REACH:]
                accv[h, new] = part_v[REACH:]
            dqo[rows, cols] = dot(low_g, k[keys, cols], TN).astype(BF16)

    @pl.when(has_prev)
    def _():
        own_copy.start()
        if lead < heads:
            @pl.loop(lead, heads)
            def _(h):
                q_copy(h).start()
                g_copy(h).start()

    @pl.when(jnp.logical_not(has_prev))
    def _():
        none = [jnp.full((1, TILE), LOW, F32), jnp.zeros((1, TILE), F32), jnp.zeros((1, TILE), F32)]
        nothing = pack(none, none)

        @pl.loop(0, heads)
        def _(h):
            st_prev[h] = nothing
            dq_in[h] = jnp.zeros((REACH, HEAD_DIM), BF16)

    @pl.when(has_next)
    def _():
        own_copy.wait_recv()

        @pl.loop(0, heads)
        def _(h):
            cols = cols_of(h)
            q_copy(h).wait_recv()
            g_copy(h).wait_recv()
            other0, other1 = unpack(st_next[h])

            def side(rows, keys_from, size, other):
                keys = slice(keys_from, keys_from + size)
                qr, gr = rq[h, rows], rg[h, rows]
                s = dot(k[keys, cols], qr, NT) * SCALE + table[h, 0:size]
                dp = dot(v[keys, cols], gr, NT)
                e, *mine = partial_stats(s, dp)
                p, sg = merged(e, dp, mine, other)
                gsum[h, 0:size] += sg
                low_p = p.astype(BF16)
                low_g = (sg * SCALE).astype(BF16)
                acck[h, keys] += dot(low_g, qr, NN)
                accv[h, keys] += dot(low_p, gr, NN)
                dq_out[h, rows] = dot(low_g, k[keys, cols], TN).astype(BF16)
                return mine

            mine0 = side(slice(0, TILE), tok - REACH, REACH, other0)
            mine1 = side(slice(TILE, REACH), tok - TILE, TILE, other1)
            st_half[h] = pack(mine0, mine1)
            half_copy(h).start()

        @pl.loop(0, half_heads)
        def _(h):
            dq_copy(h).start()

    @pl.loop(0, heads)
    def _(h):
        cols = cols_of(h)

        @pl.when(has_prev)
        def _():
            half_copy(h).wait_recv()

        other0, other1 = unpack(st_prev[h])
        mine0, mine1 = unpack(st_own[h])
        p0, sg0 = merged(es[h, 0:TILE], dps[h, 0:TILE], mine0, other0)
        p1, sg1 = merged(es[h, TILE:SPAN], dps[h, TILE:SPAN], mine1, other1)
        sums = gsum[h]
        far = sums[:TILE]
        mid = sums[TILE:REACH] + sg1[:TILE]
        diag = sums[REACH:] + sg1[TILE:] + sg0
        clipped = jnp.sum(far + jnp.where(beyond, mid, 0.0), axis=0, keepdims=True)
        clipped = jnp.sum(clipped, axis=1, keepdims=True)
        both = jnp.concatenate([diag, jnp.where(beyond, 0.0, mid)], axis=1)
        b0[pl.ds(h, 1), :] = skew_sum(both) + jnp.where(lane == BUCKETS - 1, clipped, 0.0)

        gl0, gl1 = (sg0 * SCALE).astype(BF16), (sg1 * SCALE).astype(BF16)
        q0, q1 = q[0:TILE, cols], q[TILE:REACH, cols]
        g0, g1 = g[0:TILE, cols], g[TILE:REACH, cols]
        for acc, out, a0, a1, x0, x1 in (
            (acck, dko, gl0, gl1, q0, q1), (accv, dvo, p0.astype(BF16), p1.astype(BF16), g0, g1)):
            second = dot(a1, x1, NN)
            out[0:TILE, cols] = (acc[h, 0:TILE] + second[:TILE] + dot(a0, x0, NN)).astype(BF16)
            out[TILE:REACH, cols] = (acc[h, TILE:REACH] + second[TILE:]).astype(BF16)
            out[REACH:tok, cols] = acc[h, REACH:tok].astype(BF16)
        dq_loc[h, 0:TILE] = dot(gl0, k[0:TILE, cols], TN)
        dq_loc[h, TILE:REACH] = dot(gl1, k[0:REACH, cols], TN)

    dk_store = pltpu.make_async_copy(dko, dk_hbm.at[0], kv_sem.at[0])
    dv_store = pltpu.make_async_copy(dvo, dv_hbm.at[0], kv_sem.at[1])

    def copies(src, slots, send, recv, index, count, device):
        outgoing, incoming = [], []
        for d in range(1, count):
            peer = lax.rem(index + d, count)
            outgoing.append(pltpu.make_async_remote_copy(
                src, slots.at[index], send.at[d - 1], recv.at[index],
                device_id=device(peer), device_id_type=MESH))
            incoming.append(pltpu.make_async_remote_copy(
                src, slots.at[peer], send.at[d - 1], recv.at[peer],
                device_id=device(peer), device_id_type=MESH))
        return outgoing, incoming

    out1, in1 = copies(b0, slots1, e1_s, e1_r, low, low_n, lambda p: {"sp": high * low_n + p})
    out2, in2 = copies(b1, slots2, e2_s, e2_r, high, high_n, lambda p: {"sp": p * low_n + low})
    out3, in3 = copies(b2, slots3, e3_s, e3_r, tp, tp_n, lambda p: {"tp": p})

    for copy in out1:
        copy.start()
    slots1[low] = b0[...]
    dk_store.start()
    dv_store.start()

    @pl.when(has_next)
    def _():
        @pl.loop(half_heads, heads - 1)
        def _(h):
            dq_copy(h).start()

    for copy in in1:
        copy.wait_recv()
    total = slots1[0]
    for i in range(1, low_n):
        total += slots1[i]
    b1[...] = total
    for copy in out2:
        copy.start()
    slots2[high] = total

    @pl.when(has_next)
    def _():
        dq_copy(heads - 1).start()

    for copy in in2:
        copy.wait_recv()
    total = slots2[0]
    for i in range(1, high_n):
        total += slots2[i]
    b2[...] = total
    for copy in out3:
        copy.start()
    slots3[tp] = total

    def dq_store(h):
        cols = cols_of(h)
        return pltpu.make_async_copy(dqo.at[:, cols], dq_hbm.at[0, :, cols], dqo_sem.at[h])

    @pl.loop(0, heads)
    def _(h):
        @pl.when(has_prev)
        def _():
            dq_copy(h).wait_recv()

        dqo[0:REACH, cols_of(h)] = (dq_loc[h] + dq_in[h].astype(F32)).astype(BF16)
        dq_store(h).start()

    for copy in in3:
        copy.wait_recv()
    for i in range(tp_n):
        bias_ref[i * heads : (i + 1) * heads, :] = slots3[i, 0:heads, 0:BUCKETS]

    for copy in out1 + out2 + out3:
        copy.wait_send()

    @pl.when(has_prev)
    def _():
        own_copy.wait_send()

        @pl.loop(0, heads)
        def _(h):
            q_copy(h).wait_send()
            g_copy(h).wait_send()

    @pl.when(has_next)
    def _():
        @pl.loop(0, heads)
        def _(h):
            half_copy(h).wait_send()
            dq_copy(h).wait_send()

    dk_store.wait()
    dv_store.wait()

    @pl.loop(0, heads)
    def _(h):
        dq_store(h).wait()


def local(sp_n, tp_n, queries, keys, values, rel_bias, out_grad):
    seq_count, tok, width = queries.shape
    heads = width // HEAD_DIM
    low_n = max(d for d in range(1, sp_n + 1) if sp_n % d == 0 and d * d <= sp_n)
    high_n = sp_n // low_n
    pad = -(-heads // 8) * 8
    any_spec = pl.BlockSpec(memory_space=pl.ANY)
    vmem_spec = pl.BlockSpec(memory_space=pltpu.VMEM)
    block = jax.ShapeDtypeStruct(queries.shape, BF16)
    dma = pltpu.SemaphoreType.DMA
    big = pltpu.VMEM((tok, width), BF16)
    span = pltpu.VMEM((heads, SPAN, TILE), F32)
    acc = pltpu.VMEM((heads, tok, HEAD_DIM), F32)
    stats = pltpu.VMEM((heads, 8, TILE), F32)
    halo = pltpu.VMEM((heads, REACH, HEAD_DIM), BF16)
    row = pltpu.VMEM((pad, LANES), F32)
    return pl.pallas_call(
        functools.partial(kernel, sp_n, tp_n, low_n, heads, tok),
        out_shape=(block, block, block, jax.ShapeDtypeStruct((heads * tp_n, BUCKETS), F32)),
        in_specs=[any_spec] * 4 + [vmem_spec],
        out_specs=(any_spec, any_spec, any_spec, vmem_spec),
        scratch_shapes=[big] * 7 + [halo, halo, row, span, span, acc, acc, span, span]
        + [stats] * 4
        + [pltpu.VMEM((heads, REACH, HEAD_DIM), F32), halo, halo]
        + [row, row, row]
        + [pltpu.VMEM((n, pad, LANES), F32) for n in (low_n, high_n, tp_n)]
        + [dma((4,))] + [dma((heads,))] * 4 + [dma((1,))] * 2 + [dma((heads,))] * 4
        + [dma((low_n,))] * 2 + [dma((high_n,))] * 2 + [dma((tp_n,))] * 2
        + [dma((2,)), dma((heads,))],
        compiler_params=pltpu.CompilerParams(
            collective_id=0, has_side_effects=True, vmem_limit_bytes=56 * 1024 * 1024
        ),
    )(queries, keys, values, out_grad, rel_bias)


def solution(mesh):
    split = P(None, "sp", "tp")
    return jax.shard_map(
        functools.partial(local, mesh.shape["sp"], mesh.shape["tp"]),
        mesh=mesh,
        in_specs=(split, split, split, P("tp", None), split),
        out_specs=(split, split, split, P()),
        check_vma=False,
    )
```

time: 185 us -> 57.4 us (0.31)
  blocking collectives: 54.4 us -> 0 us
  Pallas kernels: 0 us -> 51.5 us
  local copies, waits for them, and re-layouts: 52.7 us -> 5.04 us
  matrix products: 27.5 us -> 0 us
  other arithmetic: 27.1 us -> 0 us
  starting transfers between devices: 12.1 us -> 0 us
  waiting for transfers between devices: 9.53 us -> 0 us
    psum x1 -> x0, blocking collectives: 54.4 us -> none  [local(): bias_grad = lax.psum(full_table, ('sp', 'tp'))]
    pallas_call x0 -> x1, Pallas kernels: none -> 51.5 us  [local(): pl.pallas_call(functools.partial(kernel, sp_n, tp_n, low_n, heads, tok),...]
    dot_general x27 -> x0, matrix products: 27.5 us -> none  [the longest x5 8.59 us: band_core(): jnp.einsum('sncha,snkha->snhck', q_segs, k_band[:, offset:offset + seg_co...]
    concatenate x5 -> x0, local copies, waits for them, and re-layouts: 16.2 us -> none  [the longest x1 7.01 us: band_core(): prob_grad = jnp.concatenate(prob_parts, axis=-1)]
    slice x9 -> x0, local copies, waits for them, and re-layouts: 14.7 us -> none  [the longest x1 2.25 us: local(): key_own = key_flat[:, reach:].at[:, tok_rows - reach:].add(back_k)]
    reduce_sum x4 -> x0, other arithmetic: 13.2 us -> none  [the longest x1 5.48 us: band_core(): bias_terms = jnp.sum(score_grad, axis=(0, 1))]
    ppermute x4 -> x0, starting transfers between devices: 12.1 us -> none  [from_behind(): lax.ppermute(value, axis, [(source, source + steps) for source in range(l...]
    ppermute x4 -> x0, waiting for transfers between devices: 9.53 us -> none  [from_behind(): lax.ppermute(value, axis, [(source, source + steps) for source in range(l...]
  transfers between devices with their start and end apart: 4 -> 0, of which waited for: 2 -> 0; matrix products, arithmetic and copies ran while one was open for 23% -> 0% of each run, Pallas kernels for 0% -> 0%
where the time goes in v1:
time: 57.4 us; the launch traced here: 57.2 us
  Pallas kernels  51.5 us (90%)
  local copies, waits for them, and re-layouts  5.04 us (9%)
  between operations  0.65 us (1%)
    pallas_call x1, Pallas kernels, local(): pl.pallas_call(functools.partial(kernel, sp_n, tp_n, low_n, heads, tok),...  51.5 us
    unnamed x10, local copies, waits for them, and re-layouts  5.04 us

profile of v1, /device:TPU:0, one launch (start us, length us, event | category | flops | bytes accessed | tf_op | source)
XLA Modules:
  0.0 57.2 jit_solution(11077838593773152907)
XLA Ops:
  0.6 51.5 %shard_map.84 = (bf16[1,384,1024]{2,1,0:T(8,128)(2,1)}, bf16[1,384,1024]{2,1,0:T(8,128)(2,1)}, bf16[1,384,1024]{2,1,0:T(8,128)(2,1)}, f32[16,192]{1,0:T(8,128)}) custom-call(bf16[1,384,1024]{2,1,0:T(8,128)(2,1)} %q_hbm.1, bf16[1,384,1024]{2,1,0:T(8,128)(2,1)} %k_hbm.1, bf16[1,384,1024]{2,1,0:T(8,128)(2,1)} %v_hbm.1, bf16[1,384,1024]{2,1,0:T(8,128)(2,1)} %g_hbm.1, ...), custom_call_target="tpu_custom_call" | custom-call | tf_op jit(solution)/shard_map/pallas_call | solution.py:440
  52.1 0.0 copy-start.1
  52.2 2.1 %copy.13 = bf16[1,384,1024]{2,1,0:T(8,128)(2,1)} copy(bf16[1,384,1024]{2,1,0:T(8,128)(2,1)} %get-tuple-element.8) | data formatting | bytes 1572864
  54.3 0.0 copy-done.1
  54.3 0.0 copy-start
  54.3 0.9 %copy.14 = bf16[1,384,1024]{2,1,0:T(8,128)(2,1)} copy(bf16[1,384,1024]{2,1,0:T(8,128)(2,1)S(1)} %copy-done.1) | data formatting | bytes 1572864
  55.2 0.5 copy-done
  55.7 0.0 copy-start.2
  55.7 0.9 %copy.15 = bf16[1,384,1024]{2,1,0:T(8,128)(2,1)} copy(bf16[1,384,1024]{2,1,0:T(8,128)(2,1)S(1)} %copy-done) | data formatting | bytes 1572864
  56.6 0.0 copy-done.2
  56.6 0.6 %copy.16 = f32[16,192]{1,0:T(8,128)} copy(f32[16,192]{1,0:T(8,128)S(1)} %copy-done.2) | data formatting | bytes 24576
Async XLA Ops:
  52.1 2.1 %copy-start.1 = (bf16[1,384,1024]{2,1,0:T(8,128)(2,1)S(1)}, bf16[1,384,1024]{2,1,0:T(8,128)(2,1)}, u32[]{:S(2)}) copy-start(bf16[1,384,1024]{2,1,0:T(8,128)(2,1)} %get-tuple-element.9) | copy-start | bytes 2359300
  54.3 1.4 %copy-start = (bf16[1,384,1024]{2,1,0:T(8,128)(2,1)S(1)}, bf16[1,384,1024]{2,1,0:T(8,128)(2,1)}, u32[]{:S(2)}) copy-start(bf16[1,384,1024]{2,1,0:T(8,128)(2,1)} %get-tuple-element.10) | copy-start | bytes 2359300
  55.7 0.9 %copy-start.2 = (f32[16,192]{1,0:T(8,128)S(1)}, f32[16,192]{1,0:T(8,128)}, u32[]{:S(2)}) copy-start(f32[16,192]{1,0:T(8,128)} %get-tuple-element.11) | copy-start | bytes 36868

commit v2 on v1

--- a/solution.py
+++ b/solution.py
@@ -84,22 +84,24 @@
 def kernel(
     sp_n, tp_n, low_n, heads, tok,
     q_hbm, k_hbm, v_hbm, g_hbm, rb_ref,
-    dq_hbm, dk_hbm, dv_hbm, bias_ref,
-    q, k, v, g, dqo, dko, dvo, rq, rg, rbp, table, gsum, acck, accv, es, dps,
+    dq_all, dk_all, dv_all, bias_ref,
+    q, k, v, g, rq, rg, rbp, table, gsum, acck, accv, es, dps,
     st_own, st_next, st_half, st_prev, dq_loc, dq_out, dq_in,
     b0, b1, b2, slots1, slots2, slots3,
     in_sem, q_s, q_r, g_s, g_r, so_s, so_r, sh_s, sh_r, dq_s, dq_r,
-    e1_s, e1_r, e2_s, e2_r, e3_s, e3_r, kv_sem, dqo_sem,
+    e1_s, e1_r, e2_s, e2_r, e3_s, e3_r,
 ):
     sp = lax.axis_index("sp")
+    dqo, dko, dvo = dq_all.at[0], dk_all.at[0], dv_all.at[0]
     tp = lax.axis_index("tp")
     high_n = sp_n // low_n
     low, high = lax.rem(sp, low_n), lax.div(sp, low_n)
     has_prev = sp > 0
     has_next = sp < sp_n - 1
     groups = tok // TILE
-    lead = min(3, heads)
+    lead = min(2, heads)
     half_heads = heads // 2
+    step = 2 if heads % 2 == 0 else 1
 
     def cols_of(h):
         return pl.ds(pl.multiple_of(h * HEAD_DIM, HEAD_DIM), HEAD_DIM)
@@ -177,41 +179,38 @@
     for load in loads:
         load.wait()
 
-    @pl.loop(0, heads)
-    def _(h):
+    def tiles(h, group, keys_from, size, tab_part):
         cols = cols_of(h)
+        rows = slice(group * TILE, (group + 1) * TILE)
+        keys = slice(keys_from, keys_from + size)
+        s = dot(k[keys, cols], q[rows, cols], NT) * SCALE + tab_part
+        return s, dot(v[keys, cols], g[rows, cols], NT)
+
+    def first_stats(h):
         row = rbp[pl.ds(h, 1), :]
         last = jnp.sum(jnp.where(lane == BUCKETS - 1, row, 0.0), axis=1, keepdims=True)
         both = toeplitz(row)
-        far = jnp.where(far_ok, jnp.broadcast_to(last, (TILE, TILE)), LOW)
-        mid = jnp.where(beyond, jnp.broadcast_to(last, (TILE, TILE)), both[:, TILE:])
         diag = jnp.where(diag_ok, both[:, :TILE], LOW)
-        tab = jnp.concatenate([far, mid, diag], axis=0)
-        table[h] = tab
-
-        def tiles(group, keys_from, tab_part):
-            size = tab_part.shape[0]
-            rows = slice(group * TILE, (group + 1) * TILE)
-            keys = slice(keys_from, keys_from + size)
-            s = dot(k[keys, cols], q[rows, cols], NT) * SCALE + tab_part
-            dp = dot(v[keys, cols], g[rows, cols], NT)
-            return s, dp
-
-        s, dp = tiles(0, 0, diag)
+        table[h, 0:TILE] = jnp.where(far_ok, jnp.broadcast_to(last, (TILE, TILE)), LOW)
+        table[h, TILE:REACH] = jnp.where(beyond, jnp.broadcast_to(last, (TILE, TILE)), both[:, TILE:])
+        table[h, REACH:SPAN] = diag
+        s, dp = tiles(h, 0, 0, TILE, diag)
         e0, *st0 = partial_stats(s, dp)
         es[h, 0:TILE] = e0
         dps[h, 0:TILE] = dp
-        s, dp = tiles(1, 0, tab[TILE:])
+        s, dp = tiles(h, 1, 0, REACH, table[h, TILE:SPAN])
         e1, *st1 = partial_stats(s, dp)
         es[h, TILE:SPAN] = e1
         dps[h, TILE:SPAN] = dp
         st_own[h] = pack(st0, st1)
 
+    def whole_groups(h):
+        cols = cols_of(h)
         for group in range(2, groups):
             start = (group - 2) * TILE
             rows = slice(group * TILE, (group + 1) * TILE)
             keys = slice(start, start + SPAN)
-            s, dp = tiles(group, start, tab)
+            s, dp = tiles(h, group, start, SPAN, table[h])
             e, m, l, d = partial_stats(s, dp)
             inv = 1.0 / l
             p = e * inv
@@ -234,6 +233,18 @@
                 accv[h, new] = part_v[REACH:]
             dqo[rows, cols] = dot(low_g, k[keys, cols], TN).astype(BF16)
 
+    def each(body, ready=None):
+        @pl.loop(0, heads // step)
+        def _(i):
+            several = [i * step + j for j in range(step)]
+            if ready is not None:
+                for h in several:
+                    ready(h)
+            for h in several:
+                body(h)
+
+    each(first_stats)
+
     @pl.when(has_prev)
     def _():
         own_copy.start()
@@ -253,15 +264,18 @@
             st_prev[h] = nothing
             dq_in[h] = jnp.zeros((REACH, HEAD_DIM), BF16)
 
+    each(whole_groups)
+
     @pl.when(has_next)
     def _():
         own_copy.wait_recv()
 
-        @pl.loop(0, heads)
-        def _(h):
-            cols = cols_of(h)
+        def arrived(h):
             q_copy(h).wait_recv()
             g_copy(h).wait_recv()
+
+        def halo(h):
+            cols = cols_of(h)
             other0, other1 = unpack(st_next[h])
 
             def side(rows, keys_from, size, other):
@@ -284,18 +298,19 @@
             st_half[h] = pack(mine0, mine1)
             half_copy(h).start()
 
+        each(halo, arrived)
+
         @pl.loop(0, half_heads)
         def _(h):
             dq_copy(h).start()
 
-    @pl.loop(0, heads)
-    def _(h):
-        cols = cols_of(h)
-
+    def merged_in(h):
         @pl.when(has_prev)
         def _():
             half_copy(h).wait_recv()
 
+    def first_rows(h):
+        cols = cols_of(h)
         other0, other1 = unpack(st_prev[h])
         mine0, mine1 = unpack(st_own[h])
         p0, sg0 = merged(es[h, 0:TILE], dps[h, 0:TILE], mine0, other0)
@@ -321,8 +336,7 @@
         dq_loc[h, 0:TILE] = dot(gl0, k[0:TILE, cols], TN)
         dq_loc[h, TILE:REACH] = dot(gl1, k[0:REACH, cols], TN)
 
-    dk_store = pltpu.make_async_copy(dko, dk_hbm.at[0], kv_sem.at[0])
-    dv_store = pltpu.make_async_copy(dvo, dv_hbm.at[0], kv_sem.at[1])
+    each(first_rows, merged_in)
 
     def copies(src, slots, send, recv, index, count, device):
         outgoing, incoming = [], []
@@ -336,58 +350,52 @@
                 device_id=device(peer), device_id_type=MESH))
         return outgoing, incoming
 
-    out1, in1 = copies(b0, slots1, e1_s, e1_r, low, low_n, lambda p: {"sp": high * low_n + p})
-    out2, in2 = copies(b1, slots2, e2_s, e2_r, high, high_n, lambda p: {"sp": p * low_n + low})
+    out1, in1 = copies(b0, slots1, e1_s, e1_r, high, high_n, lambda p: {"sp": p * low_n + low})
+    out2, in2 = copies(b1, slots2, e2_s, e2_r, low, low_n, lambda p: {"sp": high * low_n + p})
     out3, in3 = copies(b2, slots3, e3_s, e3_r, tp, tp_n, lambda p: {"tp": p})
 
     for copy in out1:
         copy.start()
-    slots1[low] = b0[...]
-    dk_store.start()
-    dv_store.start()
-
-    @pl.when(has_next)
-    def _():
-        @pl.loop(half_heads, heads - 1)
-        def _(h):
-            dq_copy(h).start()
+    slots1[high] = b0[...]
 
     for copy in in1:
         copy.wait_recv()
     total = slots1[0]
-    for i in range(1, low_n):
+    for i in range(1, high_n):
         total += slots1[i]
     b1[...] = total
     for copy in out2:
         copy.start()
-    slots2[high] = total
+    slots2[low] = total
 
     @pl.when(has_next)
     def _():
-        dq_copy(heads - 1).start()
+        @pl.loop(half_heads, heads)
+        def _(h):
+            dq_copy(h).start()
+
+    def finish(lo, hi):
+        @pl.loop(lo, hi)
+        def _(h):
+            @pl.when(has_prev)
+            def _():
+                dq_copy(h).wait_recv()
+
+            dqo[0:REACH, cols_of(h)] = (dq_loc[h] + dq_in[h].astype(F32)).astype(BF16)
+
+    finish(0, half_heads)
 
     for copy in in2:
         copy.wait_recv()
     total = slots2[0]
-    for i in range(1, high_n):
+    for i in range(1, low_n):
         total += slots2[i]
     b2[...] = total
     for copy in out3:
         copy.start()
     slots3[tp] = total
 
-    def dq_store(h):
-        cols = cols_of(h)
-        return pltpu.make_async_copy(dqo.at[:, cols], dq_hbm.at[0, :, cols], dqo_sem.at[h])
-
-    @pl.loop(0, heads)
-    def _(h):
-        @pl.when(has_prev)
-        def _():
-            dq_copy(h).wait_recv()
-
-        dqo[0:REACH, cols_of(h)] = (dq_loc[h] + dq_in[h].astype(F32)).astype(BF16)
-        dq_store(h).start()
+    finish(half_heads, heads)
 
     for copy in in3:
         copy.wait_recv()
@@ -412,13 +420,6 @@
         def _(h):
             half_copy(h).wait_send()
             dq_copy(h).wait_send()
-
-    dk_store.wait()
-    dv_store.wait()
-
-    @pl.loop(0, heads)
-    def _(h):
-        dq_store(h).wait()
 
 
 def local(sp_n, tp_n, queries, keys, values, rel_bias, out_grad):
@@ -429,7 +430,6 @@
     pad = -(-heads // 8) * 8
     any_spec = pl.BlockSpec(memory_space=pl.ANY)
     vmem_spec = pl.BlockSpec(memory_space=pltpu.VMEM)
-    block = jax.ShapeDtypeStruct(queries.shape, BF16)
     dma = pltpu.SemaphoreType.DMA
     big = pltpu.VMEM((tok, width), BF16)
     span = pltpu.VMEM((heads, SPAN, TILE), F32)
@@ -439,19 +439,18 @@
     row = pltpu.VMEM((pad, LANES), F32)
     return pl.pallas_call(
         functools.partial(kernel, sp_n, tp_n, low_n, heads, tok),
-        out_shape=(block, block, block, jax.ShapeDtypeStruct((heads * tp_n, BUCKETS), F32)),
+        out_shape=(pltpu.VMEM(queries.shape, BF16),) * 3 + ( jax.ShapeDtypeStruct((heads * tp_n, BUCKETS), F32),),
         in_specs=[any_spec] * 4 + [vmem_spec],
-        out_specs=(any_spec, any_spec, any_spec, vmem_spec),
-        scratch_shapes=[big] * 7 + [halo, halo, row, span, span, acc, acc, span, span]
+        out_specs=(vmem_spec,) * 4,
+        scratch_shapes=[big] * 4 + [halo, halo, row, span, span, acc, acc, span, span]
         + [stats] * 4
         + [pltpu.VMEM((heads, REACH, HEAD_DIM), F32), halo, halo]
         + [row, row, row]
-        + [pltpu.VMEM((n, pad, LANES), F32) for n in (low_n, high_n, tp_n)]
+        + [pltpu.VMEM((n, pad, LANES), F32) for n in (high_n, low_n, tp_n)]
         + [dma((4,))] + [dma((heads,))] * 4 + [dma((1,))] * 2 + [dma((heads,))] * 4
-        + [dma((low_n,))] * 2 + [dma((high_n,))] * 2 + [dma((tp_n,))] * 2
-        + [dma((2,)), dma((heads,))],
+        + [dma((high_n,))] * 2 + [dma((low_n,))] * 2 + [dma((tp_n,))] * 2,
         compiler_params=pltpu.CompilerParams(
-            collective_id=0, has_side_effects=True, vmem_limit_bytes=56 * 1024 * 1024
+            collective_id=0, has_side_effects=True, vmem_limit_bytes=64_500_000
         ),
     )(queries, keys, values, out_grad, rel_bias)
 

time: 57.4 us -> 51.3 us (0.89)
  Pallas kernels: 51.5 us -> 46.8 us
  local copies, waits for them, and re-layouts: 5.04 us -> 3.25 us
    pallas_call x1, Pallas kernels: 51.5 us -> 46.8 us  [local(): pl.pallas_call(functools.partial(kernel, sp_n, tp_n, low_n, heads, tok),...]
    unnamed x10 -> x6, local copies, waits for them, and re-layouts: 5.04 us -> 3.25 us
where the time goes in v2:
time: 51.3 us; the launch traced here: 50.7 us
  Pallas kernels  46.8 us (91%)
  local copies, waits for them, and re-layouts  3.25 us (6%)
  between operations  0.64 us (1%)
    pallas_call x1, Pallas kernels, local(): pl.pallas_call(functools.partial(kernel, sp_n, tp_n, low_n, heads, tok),...  46.8 us
    unnamed x6, local copies, waits for them, and re-layouts  3.25 us

profile of v2, /device:TPU:0, one launch (start us, length us, event | category | flops | bytes accessed | tf_op | source)
XLA Modules:
  0.0 50.7 jit_solution(14596062369350024933)
XLA Ops:
  0.6 46.8 %shard_map.84 = (bf16[1,384,1024]{2,1,0:T(8,128)(2,1)S(1)}, bf16[1,384,1024]{2,1,0:T(8,128)(2,1)S(1)}, bf16[1,384,1024]{2,1,0:T(8,128)(2,1)S(1)}, f32[16,192]{1,0:T(8,128)}) custom-call(bf16[1,384,1024]{2,1,0:T(8,128)(2,1)} %q_hbm.1, bf16[1,384,1024]{2,1,0:T(8,128)(2,1)} %k_hbm.1, bf16[1,384,1024]{2,1,0:T(8,128)(2,1)} %v_hbm.1, bf16[1,384,1024]{2,1,0:T(8,128)(2,1)} %g_hbm.1, ...), custom_call_target="tpu_custom_call" | custom-call | tf_op jit(solution)/shard_map/pallas_call | solution.py:440
  47.4 0.9 %copy.13 = bf16[1,384,1024]{2,1,0:T(8,128)(2,1)} copy(bf16[1,384,1024]{2,1,0:T(8,128)(2,1)S(1)} %get-tuple-element.4) | data formatting | bytes 1572864
  48.3 0.9 %copy.14 = bf16[1,384,1024]{2,1,0:T(8,128)(2,1)} copy(bf16[1,384,1024]{2,1,0:T(8,128)(2,1)S(1)} %get-tuple-element.5) | data formatting | bytes 1572864
  49.2 0.0 copy-start
  49.2 0.9 %copy.15 = bf16[1,384,1024]{2,1,0:T(8,128)(2,1)} copy(bf16[1,384,1024]{2,1,0:T(8,128)(2,1)S(1)} %get-tuple-element.6) | data formatting | bytes 1572864
  50.1 0.0 copy-done
  50.1 0.6 %copy.16 = f32[16,192]{1,0:T(8,128)} copy(f32[16,192]{1,0:T(8,128)S(1)} %copy-done) | data formatting | bytes 24576
Async XLA Ops:
  49.2 0.9 %copy-start = (f32[16,192]{1,0:T(8,128)S(1)}, f32[16,192]{1,0:T(8,128)}, u32[]{:S(2)}) copy-start(f32[16,192]{1,0:T(8,128)} %get-tuple-element.15) | copy-start | bytes 36868

commit v3 on v2

--- a/solution.py
+++ b/solution.py
@@ -422,6 +422,15 @@
             dq_copy(h).wait_send()
 
 
+def store(*refs):
+    sem = refs[-1]
+    copies = [pltpu.make_async_copy(refs[i], refs[4 + i], sem.at[i]) for i in range(4)]
+    for copy in copies:
+        copy.start()
+    for copy in copies:
+        copy.wait()
+
+
 def local(sp_n, tp_n, queries, keys, values, rel_bias, out_grad):
     seq_count, tok, width = queries.shape
     heads = width // HEAD_DIM
@@ -437,9 +446,10 @@
     stats = pltpu.VMEM((heads, 8, TILE), F32)
     halo = pltpu.VMEM((heads, REACH, HEAD_DIM), BF16)
     row = pltpu.VMEM((pad, LANES), F32)
-    return pl.pallas_call(
+    held = pl.pallas_call(
         functools.partial(kernel, sp_n, tp_n, low_n, heads, tok),
-        out_shape=(pltpu.VMEM(queries.shape, BF16),) * 3 + ( jax.ShapeDtypeStruct((heads * tp_n, BUCKETS), F32),),
+        out_shape=(pltpu.VMEM(queries.shape, BF16),) * 3
+        + (pltpu.VMEM((heads * tp_n, BUCKETS), F32),),
         in_specs=[any_spec] * 4 + [vmem_spec],
         out_specs=(vmem_spec,) * 4,
         scratch_shapes=[big] * 4 + [halo, halo, row, span, span, acc, acc, span, span]
@@ -453,6 +463,14 @@
             collective_id=0, has_side_effects=True, vmem_limit_bytes=64_500_000
         ),
     )(queries, keys, values, out_grad, rel_bias)
+    return pl.pallas_call(
+        store,
+        out_shape=tuple(jax.ShapeDtypeStruct(x.shape, x.dtype) for x in held),
+        in_specs=[any_spec] * 4,
+        out_specs=(any_spec,) * 4,
+        scratch_shapes=[dma((4,))],
+        compiler_params=pltpu.CompilerParams(vmem_limit_bytes=1024 * 1024),
+    )(*held)
 
 
 def solution(mesh):

time: 51.3 us -> 48.9 us (0.953)
  local copies, waits for them, and re-layouts: 3.25 us -> 0 us
  Pallas kernels: 46.8 us -> 47.6 us
    unnamed x6 -> x0, local copies, waits for them, and re-layouts: 3.25 us -> none
    pallas_call x0 -> x1, Pallas kernels: none -> 1.44 us  [local(): pl.pallas_call(store, out_shape=tuple((jax.ShapeDtypeStruct(x.shape, x.dt...]
    pallas_call x1, Pallas kernels: 46.8 us -> 46.2 us  [local(): pl.pallas_call(functools.partial(kernel, sp_n, tp_n, low_n, heads, tok),...]
where the time goes in v3:
time: 48.9 us; the launch traced here: 48.3 us
  Pallas kernels  47.6 us (97%)
  between operations  0.64 us (1%)
    pallas_call x1, Pallas kernels, local(): pl.pallas_call(functools.partial(kernel, sp_n, tp_n, low_n, heads, tok),...  46.2 us
    pallas_call x1, Pallas kernels, local(): pl.pallas_call(store, out_shape=tuple((jax.ShapeDtypeStruct(x.shape, x.dt...  1.44 us

profile of v3, /device:TPU:0, one launch (start us, length us, event | category | flops | bytes accessed | tf_op | source)
XLA Modules:
  0.0 48.3 jit_solution(4875435685659716641)
XLA Ops:
  0.6 46.2 %shard_map.84 = (bf16[1,384,1024]{2,1,0:T(8,128)(2,1)S(1)}, bf16[1,384,1024]{2,1,0:T(8,128)(2,1)S(1)}, bf16[1,384,1024]{2,1,0:T(8,128)(2,1)S(1)}, f32[16,192]{1,0:T(8,128)S(1)}) custom-call(bf16[1,384,1024]{2,1,0:T(8,128)(2,1)} %q_hbm.1, bf16[1,384,1024]{2,1,0:T(8,128)(2,1)} %k_hbm.1, bf16[1,384,1024]{2,1,0:T(8,128)(2,1)} %v_hbm.1, ...), custom_call_target="tpu_custom_call" | custom-call | tf_op jit(solution)/shard_map/pallas_call | solution.py:449
  46.8 1.4 %shard_map.85 = (bf16[1,384,1024]{2,1,0:T(8,128)(2,1)}, bf16[1,384,1024]{2,1,0:T(8,128)(2,1)}, bf16[1,384,1024]{2,1,0:T(8,128)(2,1)}, f32[16,192]{1,0:T(8,128)}) custom-call(bf16[1,384,1024]{2,1,0:T(8,128)(2,1)S(1)} %get-tuple-element.8.refs_0_, bf16[1,384,1024]{2,1,0:T(8,128)(2,1)S(1)} %get-tuple-element.9.refs_1_, ...), custom_call_target="tpu_custom_call" | custom-call | tf_op jit(solution)/shard_map/pallas_call | solution.py:466
